TPU v7x, 128 devices: a whole 4x4x4 slice. The times are simulated.
128 devices in a mesh: sp: 16 (over z, x), tp: 8 (over y, core).
Axes of the slice: x: 4, y: 4, z: 4, core: 2. Of those that a mesh axis runs over, the one named last changes fastest.
Arguments:
- target: bfloat16 [8192, 4096], P(('sp', 'tp')), may hold values from -0.07 to 0.07
- source: bfloat16 [16384, 4096], P(('sp', 'tp')), may hold values from -0.035 to 0.035
- gain_target: float32 [4096], replicated, may hold values from 0.1 to 1.9
- gain_source: float32 [4096], replicated, may hold values from 0.1 to 1.9
- w_query: bfloat16 [4096, 1024], P(None, 'tp'), may hold values from -1 to 1
- w_key: bfloat16 [4096, 512], replicated, may hold values from -1 to 1
- w_value: bfloat16 [4096, 512], replicated, may hold values from -0.09375 to 0.09375
- w_out: bfloat16 [1024, 4096], P('tp'), may hold values from -0.1875 to 0.1875
- grad_output: bfloat16 [8192, 4096], P(('sp', 'tp')), may hold values from -6 to 6
Outputs:
- grad_target: float32 [8192, 4096], P(('sp', 'tp'))
- grad_source: float32 [16384, 4096], P(('sp', 'tp'))
- grad_out_proj: float32 [1024, 4096], P('tp')
All inputs are finite; a program needn't handle non-finite values.
Results may differ from a plain program's by a relative error of at most 0.028.
Values may be sent and summed in bfloat16 or wider, within the bound.
No kernel may reach another device: no remote copies, remote signals or barrier semaphores. Data moves between devices by JAX's collectives and lax.ppermute only.
A program may use at most 128 MiB of HBM per device.

v0:
```python
import math
import jax
import jax.numpy as jnp
from jax import lax
from jax.sharding import PartitionSpec as P

HD = 64
EPS = 1e-06


def sent_together(arrays, axis, dim, along):
    both = jnp.concatenate(arrays, axis=along)
    whole, at, finished = (lax.all_gather(both, axis, axis=dim, tiled=True), 0, [])
    for a in arrays:
        finished.append(lax.slice_in_dim(whole, at, at + a.shape[along], axis=along))
        at += a.shape[along]
    return tuple(finished)


def normalize(matrix, scaling):
    widened = matrix.astype(jnp.float32)
    factor = lax.rsqrt(jnp.mean(widened * widened, axis=-1, keepdims=True) + EPS)
    return (widened * factor * scaling).astype(jnp.bfloat16)


def norm_back(matrix, scaling, upstream):
    widened = matrix.astype(jnp.float32)
    factor = lax.rsqrt(jnp.mean(widened * widened, axis=-1, keepdims=True) + EPS)
    weighted = upstream * scaling
    inner = jnp.mean(widened * weighted, axis=-1, keepdims=True)
    return factor * weighted - widened * factor * factor * factor * inner


def score_block(queries, key_block, score_scale):
    return (
        jnp.einsum(
            "tkgd,skd->kgts", queries, key_block[:, :, 0], preferred_element_type=jnp.float32
        )
        * score_scale
    )


def split_arrived(arrived, key_count):
    row_count = arrived.shape[0]
    block_size = math.gcd(row_count, 1024)
    return (arrived.reshape(row_count // block_size, block_size, key_count, 2, HD), block_size)


def shards(target, source, gain_target, gain_source, w_query, w_key, w_value, w_out, grad_output):
    contract_last = (((1,), (1,)), ((), ()))
    across = lax.axis_size("tp")
    heads_all = w_key.shape[1] // HD
    key_count = heads_all // across
    query_count = w_query.shape[1] // HD
    group_size = query_count // key_count
    score_scale = float(HD) ** (-0.5)
    normed_target = normalize(target, gain_target)
    normed_source = normalize(source, gain_source)
    gathered_target, gathered_grad = sent_together((normed_target, grad_output), "tp", 0, 1)
    query = jnp.dot(gathered_target, w_query, preferred_element_type=jnp.float32).astype(
        jnp.bfloat16
    )
    head_grads = lax.dot_general(
        gathered_grad, w_out, contract_last, preferred_element_type=jnp.float32
    ).astype(jnp.bfloat16)
    row_count = query.shape[0]
    queries = query.reshape(row_count, key_count, group_size, HD)
    grad_heads = head_grads.reshape(row_count, key_count, group_size, HD)
    w_both = jnp.stack(
        [w_key.reshape(-1, heads_all, HD), w_value.reshape(-1, heads_all, HD)], axis=2
    )
    w_both = w_both.reshape(w_key.shape[0], heads_all * 2 * HD)
    pairs = jnp.dot(normed_source, w_both, preferred_element_type=jnp.float32).astype(jnp.bfloat16)
    own_pairs = lax.all_to_all(pairs, "tp", split_axis=1, concat_axis=0, tiled=True)
    start_max = jnp.full((key_count, group_size, row_count), -jnp.inf, jnp.float32)
    start_sum = jnp.zeros((key_count, group_size, row_count), jnp.float32)
    start_acc = jnp.zeros((row_count, key_count, group_size, HD), jnp.float32)
    blocks, block_size = split_arrived(
        lax.all_gather(own_pairs, "sp", axis=0, tiled=True), key_count
    )

    def absorb_advance(status, key_block):
        maxima, totals, accum = status
        scores = score_block(queries, key_block, score_scale)
        new_max = jnp.maximum(maxima, jnp.max(scores, axis=-1))
        shrink = jnp.exp(maxima - new_max)
        weights = jnp.exp(scores - new_max[..., None])
        totals = totals * shrink + jnp.sum(weights, axis=-1)
        partial_value = jnp.einsum(
            "kgts,skd->tkgd",
            weights.astype(jnp.bfloat16),
            key_block[:, :, 1],
            preferred_element_type=jnp.float32,
        )
        accum = accum * jnp.transpose(shrink, (2, 0, 1))[..., None] + partial_value
        return ((new_max, totals, accum), None)

    result, _ = lax.scan(absorb_advance, (start_max, start_sum, start_acc), blocks)
    maxima, totals, accum = result
    attn_heads = (accum / jnp.transpose(totals, (2, 0, 1))[..., None]).astype(jnp.bfloat16)
    delta_sum = jnp.sum(grad_heads.astype(jnp.float32) * attn_heads.astype(jnp.float32), axis=-1)
    delta_sum = jnp.transpose(delta_sum, (1, 2, 0))
    all_rows = own_pairs.shape[0] * lax.axis_size("sp")
    start_grad = jnp.zeros((row_count, key_count, group_size, HD), jnp.float32)
    start_pairs = jnp.zeros((all_rows, key_count * 2 * HD), jnp.float32)
    blocks, block_size = split_arrived(
        lax.all_gather(own_pairs, "sp", axis=0, tiled=True), key_count
    )

    def collect_advance(status, bundle):
        query_grad, pair_store = status
        key_block, position = bundle
        scores = score_block(queries, key_block, score_scale)
        attend = jnp.exp(scores - maxima[..., None]) / totals[..., None]
        grad_attend = jnp.einsum(
            "tkgd,skd->kgts", grad_heads, key_block[:, :, 1], preferred_element_type=jnp.float32
        )
        mixed = (attend * (grad_attend - delta_sum[..., None]) * score_scale).astype(jnp.bfloat16)
        query_grad = query_grad + jnp.einsum(
            "kgts,skd->tkgd", mixed, key_block[:, :, 0], preferred_element_type=jnp.float32
        )
        grad_key = jnp.einsum("kgts,tkgd->skd", mixed, queries, preferred_element_type=jnp.float32)
        grad_value = jnp.einsum(
            "kgts,tkgd->skd",
            attend.astype(jnp.bfloat16),
            grad_heads,
            preferred_element_type=jnp.float32,
        )
        stacked = jnp.stack([grad_key, grad_value], axis=2).reshape(block_size, key_count * 2 * HD)
        where_rows = position * block_size
        pair_store = lax.dynamic_update_slice_in_dim(pair_store, stacked, where_rows, 0)
        return ((query_grad, pair_store), None)

    positions = jnp.arange(blocks.shape[0], dtype=jnp.int32)
    result, _ = lax.scan(collect_advance, (start_grad, start_pairs), (blocks, positions))
    query_grad, pair_store = result
    pair_grads = lax.psum_scatter(
        pair_store.astype(jnp.bfloat16), "sp", scatter_dimension=0, tiled=True
    )
    grad_query = query_grad.astype(jnp.bfloat16).reshape(row_count, query_count * HD)
    pair_rows = lax.all_to_all(pair_grads, "tp", split_axis=0, concat_axis=1, tiled=True)
    grad_sn = lax.dot_general(pair_rows, w_both, contract_last, preferred_element_type=jnp.float32)
    grad_source = norm_back(source, gain_source, grad_sn)
    attention = attn_heads.reshape(row_count, query_count * HD)
    proj_part = lax.dot_general(
        attention, gathered_grad, (((0,), (0,)), ((), ())), preferred_element_type=jnp.float32
    )
    grad_out_proj = lax.psum(proj_part.astype(jnp.bfloat16), "sp").astype(jnp.float32)
    grad_xn = lax.psum_scatter(
        lax.dot_general(
            grad_query, w_query, contract_last, preferred_element_type=jnp.float32
        ).astype(jnp.bfloat16),
        "tp",
        scatter_dimension=0,
        tiled=True,
    ).astype(jnp.float32)
    grad_target = norm_back(target, gain_target, grad_xn)
    return (grad_target, grad_source, grad_out_proj)


def solution(mesh):
    return jax.shard_map(
        shards,
        mesh=mesh,
        in_specs=(
            P(("sp", "tp"), None),
            P(("sp", "tp"), None),
            P(),
            P(),
            P(None, "tp"),
            P(),
            P(),
            P("tp", None),
            P(("sp", "tp"), None),
        ),
        out_specs=(P(("sp", "tp"), None), P(("sp", "tp"), None), P("tp", None)),
        check_vma=False,
    )
```

profile of v0, /device:TPU:0, one launch (start us, length us, event | category | flops | bytes accessed | tf_op | source)
XLA Modules:
  0.0 473.2 jit_solution(16521432054210177134)
XLA Ops:
  7.2 1.6 fusion.55
  8.8 6.5 %copy.31 = bf16[4096,512]{0,1:T(8,128)(2,1)} copy(bf16[4096,512]{1,0:T(8,128)(2,1)} %param.18) | data formatting | bytes 8388608 | tf_op args[5]
  15.3 6.4 %copy.32 = bf16[4096,512]{0,1:T(8,128)(2,1)} copy(bf16[4096,512]{1,0:T(8,128)(2,1)} %param.19) | data formatting | bytes 8388608 | tf_op args[6]
  21.7 7.4 %pad_maximum_fusion.1 = bf16[4096,8,2,64]{0,3,1,2:T(8,128)(2,1)} fusion(bf16[4096,8,1,64]{0,3,1,2:T(8,128)(2,1)} %bitcast.250, bf16[4096,8,1,64]{0,3,1,2:T(8,128)(2,1)} %bitcast.249), kind=kLoop, calls=%fused_computation.49 | loop fusion | flops 4194304 | bytes 16777216 | tf_op jit(solution)/shard_map/stack | solution.py:69
  29.1 7.8 %copy.33 = bf16[4096,8,2,64]{0,3,2,1:T(8,128)(2,1)} copy(bf16[4096,8,2,64]{0,3,1,2:T(8,128)(2,1)} %pad_maximum_fusion.1) | data formatting | bytes 16777216 | tf_op jit(solution)/shard_map/stack | solution.py:69
  37.0 6.4 %fusion.59 = bf16[16,8,8,128]{3,2,1,0:T(8,128)(2,1)S(1)} fusion(bf16[4096,1024]{0,1:T(8,128)(2,1)} %bitcast.246, bf16[128,4096]{1,0:T(8,128)(2,1)S(1)} %copy-done.1, f32[4096]{0:T(1024)S(1)} %copy-done.6, f32[128]{0:T(128)S(1)} %add_rsqrt_fusion), kind=kOutput, calls=%fused_computation.75 | convolution fusion | flops 1075970048 | bytes 9716224 | tf_op jit(solution)/shard_map/dot_general | solution.py:73
  43.4 12.0 %all_to_all.38 = bf16[128,8,128]{2,0,1:T(8,128)(2,1)} all-to-all(bf16[128,8,128]{2,0,1:T(8,128)(2,1)S(1)} %bitcast.259), channel_id=1, replica_groups=mesh['sp'=16,'tp'=8] {'tp'}, dimensions={1} | all-to-all | bytes 524288 | tf_op jit(solution)/shard_map/all_to_all | solution.py:74
  55.9 1.0 pad_maximum_fusion.2
  57.3 50.2 %all-gather.3.cloned.1.call-done = bf16[16384,128]{1,0:T(8,128)(2,1)} async-done(((bf16[1024,128]{1,0:T(8,128)(2,1)}), bf16[16384,128]{1,0:T(8,128)(2,1)}) %all-gather.3.cloned.1.call-update) | async-done | bytes 4194320 | tf_op jit(solution)/shard_map/all_gather | solution.py:107
  107.4 14.7 %reshape.168 = bf16[16,1024,1,2,64]{4,3,1,0,2:T(2,128)(2,1)} reshape(bf16[16384,128]{1,0:T(8,128)(2,1)} %all-gather.3.cloned.1.call-done) | data formatting | bytes 8388608 | tf_op jit(solution)/shard_map/reshape | solution.py:46
  122.1 20.3 %copy.37 = bf16[16,1024,1,2,64]{1,4,3,2,0:T(8,128)(2,1)} copy(bf16[16,1024,1,2,64]{4,3,1,0,2:T(2,128)(2,1)} %reshape.168) | data formatting | bytes 8388608
  142.4 16.5 %all-gather.5.cloned.1.call-done = bf16[512,8192]{1,0:T(8,128)(2,1)} async-done(((bf16[64,8192]{1,0:T(8,128)(2,1)}), bf16[512,8192]{1,0:T(8,128)(2,1)}) %all-gather.5.cloned.1.call-update) | async-done | bytes 8388624 | tf_op jit(solution)/shard_map/all_gather | solution.py:13
  159.0 3.7 fusion.63
  162.7 54.3 %while.28 = (s32[]{:T(128)}, f32[1,2,512]{2,1,0:T(2,128)S(1)}, f32[1,2,512]{2,1,0:T(2,128)S(1)}, f32[512,1,2,64]{0,3,2,1:T(8,128)S(1)}, bf16[16,1024,1,2,64]{1,4...) while((s32[]{:T(128)}, f32[1,2,512]{2,1,0:T(2,128)S(1)}, ...), condition=%wide.region_5.6_spmd.clone, body=%wide.region_2.5_spmd.clone.sunk | while | flops 277026816 | bytes 14090349 | solution.py:98
  162.7 1.0 dynamic-slice_bitcast_fusion.4
  176.3 1.0 dynamic-slice_bitcast_fusion.4
  179.7 1.0 dynamic-slice_bitcast_fusion.4
  183.1 1.0 dynamic-slice_bitcast_fusion.4
  193.2 1.0 dynamic-slice_bitcast_fusion.4
  196.6 1.0 dynamic-slice_bitcast_fusion.4
  200.0 1.0 dynamic-slice_bitcast_fusion.4
  210.2 1.0 dynamic-slice_bitcast_fusion.4
  213.6 1.0 dynamic-slice_bitcast_fusion.4
  217.0 4.0 fusion.60
  221.1 3.9 convolution_convert_fusion.1
  225.0 2.2 broadcast_in_dim.6.clone
  227.3 110.4 %while.29 = (s32[]{:T(128)}, f32[512,1,2,64]{0,3,2,1:T(8,128)S(1)}, bf16[16384,128]{1,0:T(8,128)(2,1)}, bf16[16,1024,1,2,64]{1,4,3,2,0:T(8,128)(2,1)}, bf16[512,...) while((s32[]{:T(128)}, f32[512,1,2,64]{0,3,2,1:T(8,128)S(1)}, ...), condition=%wide.region_8.9_spmd.clone, body=%wide.region_7.8_spmd.clone.sunk | while | flops 679739392 | bytes 22687960 | solution.py:135
  228.5 1.0 dynamic-slice_bitcast_fusion.5
  249.2 1.0 dynamic-slice_bitcast_fusion.5
  263.0 1.0 dynamic-slice_bitcast_fusion.5
  270.8 1.0 fusion.110
  276.8 1.0 dynamic-slice_bitcast_fusion.5
  283.7 1.0 dynamic-slice_bitcast_fusion.5
  290.6 1.0 dynamic-slice_bitcast_fusion.5
  291.6 1.0 fusion.110
  297.5 1.0 dynamic-slice_bitcast_fusion.5
  304.5 1.0 dynamic-slice_bitcast_fusion.5
  311.4 1.0 dynamic-slice_bitcast_fusion.5
  318.3 1.0 dynamic-slice_bitcast_fusion.5
  337.8 3.3 convolution_convert_fusion
  341.1 2.8 convert_element_type.82
  343.9 72.7 %reduce-scatter.5.cloned.1.call-done = bf16[1024,128]{1,0:T(8,128)(2,1)} async-done(((bf16[16384,128]{1,0:T(8,128)(2,1)}), bf16[1024,128]{1,0:T(8,128)(2,1)}) %reduce-scatter.5.cloned.1.call-update) | async-done | bytes 262160 | tf_op jit(solution)/shard_map/reduce_scatter | solution.py:137
  416.7 4.3 all-to-all-start.1
  421.0 35.0 %reduce-scatter.3.cloned.1.call-done = bf16[64,4096]{1,0:T(8,128)(2,1)} async-done(((bf16[512,4096]{1,0:T(8,128)(2,1)}), bf16[64,4096]{1,0:T(8,128)(2,1)}) %reduce-scatter.3.cloned.1.call-update) | async-done | bytes 524304 | tf_op jit(solution)/shard_map/reduce_scatter | solution.py:149
  456.0 1.3 fusion.71
  457.3 2.4 fusion.69
  459.9 4.9 %fusion.56 = (f32[128]{0:T(128)S(1)}, f32[128,4096]{1,0:T(8,128)S(1)}) fusion(bf16[128,4096]{1,0:T(8,128)(2,1)S(1)} %copy-done.1, f32[4096]{0:T(1024)S(1)} %copy-done.6, bf16[128,1024]{0,1:T(8,128)(2,1)S(1)} %bitcast.256, bf16[4096,1024]{0,1:T(8,128)(2,1)} %bitcast.247), kind=kOutput, calls=%fused_computation.68 | convolution fusion | flops 1075838848 | bytes 11813376 | tf_op jit(solution)/shard_map/dot_general | solution.py:142
  464.8 1.9 fusion.54
  (292 shorter events, 133.6 us)
Async XLA Ops:
  7.2 151.8 %copy-start = (bf16[4096,128]{1,0:T(8,128)(2,1)S(1)}, bf16[4096,128]{1,0:T(8,128)(2,1)}, u32[]{:S(2)}) copy-start(bf16[4096,128]{1,0:T(8,128)(2,1)} %param.17) | copy-start | bytes 3145732
  7.2 100.2 %all-gather.3.cloned.1.call-start = ((), (), s32[]{:S(2)}) async-start(), calls=%async_computation.4 | async-start | bytes 4456448 | tf_op jit(solution)/shard_map/all_gather | solution.py:107
  29.1 7.8 %copy-start.1 = (bf16[128,4096]{1,0:T(8,128)(2,1)S(1)}, bf16[128,4096]{1,0:T(8,128)(2,1)}, u32[]{:S(2)}) copy-start(bf16[128,4096]{1,0:T(8,128)(2,1)} %param.14) | copy-start | bytes 3145732
  29.1 7.8 %copy-start.6 = (f32[4096]{0:T(1024)S(1)}, f32[4096]{0:T(1024)}, u32[]{:S(2)}) copy-start(f32[4096]{0:T(1024)} %param.16) | copy-start | bytes 49156
  36.9 18.5 %copy-start.2 = (bf16[64,4096]{1,0:T(8,128)(2,1)S(1)}, bf16[64,4096]{1,0:T(8,128)(2,1)}, u32[]{:S(2)}) copy-start(bf16[64,4096]{1,0:T(8,128)(2,1)} %param.13) | copy-start | bytes 1572868
  36.9 18.8 %copy-start.5 = (f32[4096]{0:T(1024)S(1)}, f32[4096]{0:T(1024)}, u32[]{:S(2)}) copy-start(f32[4096]{0:T(1024)} %param.15) | copy-start | bytes 49156
  36.9 19.0 %copy-start.4 = (bf16[64,4096]{1,0:T(8,128)(2,1)S(1)}, bf16[64,4096]{1,0:T(8,128)(2,1)}, u32[]{:S(2)}) copy-start(bf16[64,4096]{1,0:T(8,128)(2,1)} %param.21) | copy-start | bytes 1572868
  55.4 103.6 %all-gather.5.cloned.1.call-start = ((), (), s32[]{:S(2)}) async-start(), calls=%async_computation.5 | async-start | bytes 9437184 | tf_op jit(solution)/shard_map/all_gather | solution.py:13
  57.0 284.1 %all-reduce.2.cloned.1.call-start = ((), (), s32[]{:S(2)}) async-start(), calls=%async_computation.8 | async-start | bytes 2097152 | tf_op jit(solution)/shard_map/psum | solution.py:148
  225.0 191.7 %reduce-scatter.5.cloned.1.call-start = ((), (), s32[]{:S(2)}) async-start(), calls=%async_computation.7 | async-start | bytes 4456448 | tf_op jit(solution)/shard_map/reduce_scatter | solution.py:137
  337.7 118.2 %reduce-scatter.3.cloned.1.call-start = ((), (), s32[]{:S(2)}) async-start(), calls=%async_computation.6 | async-start | bytes 4718592 | tf_op jit(solution)/shard_map/reduce_scatter | solution.py:149
  341.1 114.9 %copy-start.3 = (bf16[64,4096]{1,0:T(8,128)(2,1)S(1)}, bf16[64,4096]{1,0:T(8,128)(2,1)}, u32[]{:S(2)}) copy-start(bf16[64,4096]{1,0:T(8,128)(2,1)} %param.13) | copy-start | bytes 1572868
  416.7 43.0 %all-to-all-start.1 = ((bf16[8,128,128]{2,1,0:T(8,128)(2,1)}), bf16[8,128,128]{2,1,0:T(8,128)(2,1)S(1)}, u32[]{:S(2)}, u32[]{:S(2)}) async-start(bf16[8,128,128]{2,1,0:T(8,128)(2,1)} %bitcast.262), calls=%async_computation.3 | async-start | bytes 524288 | tf_op jit(solution)/shard_map/all_to_all | solution.py:141
Sparse Core Ops, SparseCore 0:
  55.5 51.8 all-gather.2
  109.7 49.2 all-gather.4
  225.1 87.6 all-reduce.1
  337.9 78.7 reduce-scatter.4
  418.9 37.0 reduce-scatter.2
where the time goes:
time: 476 us; the launch traced here: 473 us
  waiting for transfers between devices  175 us (37%)
  local copies, waits for them, and re-layouts  113 us (24%)
  matrix products  112 us (24%)
  other arithmetic  31.2 us (7%)
  between operations  14 us (3%)
  blocking collectives  12 us (3%)
  loops' own time  12 us (3%)
    reduce_scatter x1, waiting for transfers between devices, shards(): lax.psum_scatter(pair_store.astype(jnp.bfloat16), 'sp', scatter_dimension...  72.7 us
    all_gather x1, waiting for transfers between devices, shards(): lax.all_gather(own_pairs, 'sp', axis=0, tiled=True)  50.2 us
    reduce_scatter x1, waiting for transfers between devices, shards(): lax.psum_scatter(lax.dot_general(grad_query, w_query, contract_last, pref...  35 us
    unnamed x17, local copies, waits for them, and re-layouts  33.2 us
    squeeze x32, local copies, waits for them, and re-layouts, shards(): lax.scan(absorb_advance, (start_max, start_sum, start_acc), blocks)  31.2 us
    dot_general x32, matrix products, score_block(): jnp.einsum('tkgd,skd->kgts', queries, key_block[:, :, 0], preferred_eleme...  27.3 us
    all_gather x1, waiting for transfers between devices, sent_together(): lax.all_gather(both, axis, axis=dim, tiled=True)  16.5 us
    reshape x1, local copies, waits for them, and re-layouts, split_arrived(): arrived.reshape(row_count // block_size, block_size, key_count, 2, HD)  14.7 us
  transfers between devices with their start and end apart: 6, of which 4 were waited for; matrix products, arithmetic and copies ran while one was open for 31% of the time, Pallas kernels for 0%

commit v1 on v0

--- a/solution.py
+++ b/solution.py
@@ -6,6 +6,19 @@
 
 HD = 64
 EPS = 1e-06
+
+
+def ring_gather(x, axis, dim):
+    ways = lax.axis_size(axis)
+    up = [(d, (d + 1) % ways) for d in range(ways)]
+    down = [(d, (d - 1) % ways) for d in range(ways)]
+    earlier, later = ([x], [x])
+    for _ in range(ways // 2):
+        earlier.append(lax.ppermute(earlier[-1], axis, up))
+    for _ in range((ways - 1) // 2):
+        later.append(lax.ppermute(later[-1], axis, down))
+    line = jnp.concatenate([*earlier[::-1], *later[1:]], axis=dim)
+    return jnp.roll(line, (lax.axis_index(axis) - ways // 2) * x.shape[dim], axis=dim)
 
 
 def sent_together(arrays, axis, dim, along):
@@ -103,9 +116,7 @@
     all_rows = own_pairs.shape[0] * lax.axis_size("sp")
     start_grad = jnp.zeros((row_count, key_count, group_size, HD), jnp.float32)
     start_pairs = jnp.zeros((all_rows, key_count * 2 * HD), jnp.float32)
-    blocks, block_size = split_arrived(
-        lax.all_gather(own_pairs, "sp", axis=0, tiled=True), key_count
-    )
+    blocks, block_size = split_arrived(ring_gather(own_pairs, "sp", 0), key_count)
 
     def collect_advance(status, bundle):
         query_grad, pair_store = status

time: 476 us -> 788 us (1.66)
  matrix products: 112 us -> 246 us
  local copies, waits for them, and re-layouts: 113 us -> 214 us
  other arithmetic: 31.2 us -> 77.1 us
  starting transfers between devices: 4.68 us -> 44.8 us
  waiting for transfers between devices: 175 us -> 160 us
    dot_general x32, matrix products: 27.3 us -> 87.3 us  [score_block(): jnp.einsum('tkgd,skd->kgts', queries, key_block[:, :, 0], preferred_eleme...]
    ppermute x0 -> x15, waiting for transfers between devices: none -> 56.6 us  [the longest x8 49.5 us: ring_gather(): earlier.append(lax.ppermute(earlier[-1], axis, up))]
    all_gather x1, waiting for transfers between devices: 50.2 us -> 0.01 us  [shards(): lax.all_gather(own_pairs, 'sp', axis=0, tiled=True)]
    dynamic_update_slice x32, local copies, waits for them, and re-layouts: 14.4 us -> 55.7 us  [collect_advance(): lax.dynamic_update_slice_in_dim(pair_store, stacked, where_rows, 0)]
    ppermute x0 -> x15, starting transfers between devices: none -> 40.1 us  [the longest x7 38.5 us: ring_gather(): later.append(lax.ppermute(later[-1], axis, down))]
    reduce_sum x16, other arithmetic: 11.2 us -> 46.2 us  [absorb_advance(): totals = totals * shrink + jnp.sum(weights, axis=-1)]
    dot_general x16, matrix products: 14.2 us -> 49.1 us  [absorb_advance(): jnp.einsum('kgts,skd->tkgd', weights.astype(jnp.bfloat16), key_block[:, :...]
    unnamed x17 -> x75, local copies, waits for them, and re-layouts: 33.2 us -> 65 us
  transfers between devices with their start and end apart: 6 -> 21, of which waited for: 4 -> 12; matrix products, arithmetic and copies ran while one was open for 31% -> 40% of each run, Pallas kernels for 0% -> 0%
where the time goes in v1:
time: 788 us; the launch traced here: 780 us
  matrix products  246 us (31%)
  local copies, waits for them, and re-layouts  214 us (27%)
  waiting for transfers between devices  160 us (20%)
  other arithmetic  77.1 us (10%)
  starting transfers between devices  44.8 us (6%)
  between operations  14.3 us (2%)
  blocking collectives  12 us (2%)
  loops' own time  11.5 us (1%)
    dot_general x32, matrix products, score_block(): jnp.einsum('tkgd,skd->kgts', queries, key_block[:, :, 0], preferred_eleme...  87.3 us
    reduce_scatter x1, waiting for transfers between devices, shards(): lax.psum_scatter(pair_store.astype(jnp.bfloat16), 'sp', scatter_dimension...  67.9 us
    unnamed x75, local copies, waits for them, and re-layouts  65 us
    dynamic_update_slice x32, local copies, waits for them, and re-layouts, collect_advance(): lax.dynamic_update_slice_in_dim(pair_store, stacked, where_rows, 0)  55.7 us
    ppermute x8, waiting for transfers between devices, ring_gather(): earlier.append(lax.ppermute(earlier[-1], axis, up))  49.5 us
    dot_general x16, matrix products, absorb_advance(): jnp.einsum('kgts,skd->tkgd', weights.astype(jnp.bfloat16), key_block[:, :...  49.1 us
    reduce_sum x16, other arithmetic, absorb_advance(): totals = totals * shrink + jnp.sum(weights, axis=-1)  46.2 us
    ppermute x7, starting transfers between devices, ring_gather(): later.append(lax.ppermute(later[-1], axis, down))  38.5 us
  transfers between devices with their start and end apart: 21, of which 12 were waited for; matrix products, arithmetic and copies ran while one was open for 40% of the time, Pallas kernels for 0%

profile of v1, /device:TPU:0, one launch (start us, length us, event | category | flops | bytes accessed | tf_op | source)
XLA Modules:
  0.0 780.3 jit_solution(10027543036886974027)
XLA Ops:
  7.2 6.6 copy.32
  13.8 6.4 copy.33
  20.2 7.4 pad_maximum_fusion.1
  27.7 7.9 %copy.34 = bf16[4096,8,2,64]{0,3,2,1:T(8,128)(2,1)} copy(bf16[4096,8,2,64]{0,3,1,2:T(8,128)(2,1)} %pad_maximum_fusion.1) | data formatting | bytes 16777216 | tf_op jit(solution)/shard_map/stack | solution.py:82
  35.8 6.3 fusion.59
  42.2 12.0 %all_to_all.38 = bf16[128,8,128]{2,0,1:T(8,128)(2,1)} all-to-all(bf16[128,8,128]{2,0,1:T(8,128)(2,1)S(1)} %bitcast.262), channel_id=1, replica_groups=mesh['sp'=16,'tp'=8] {'tp'}, dimensions={1} | all-to-all | bytes 524288 | tf_op jit(solution)/shard_map/all_to_all | solution.py:87
  57.4 10.9 %collective-permute-done = bf16[1024,128]{1,0:T(8,128)(2,1)S(1)} collective-permute-done((bf16[1024,128]{1,0:T(8,128)(2,1)}, bf16[1024,128]{1,0:T(8,128)(2,1)S(1)}, u32[]{:S(2)}, u32[]{:S(2)}) %collective-permute-start) | collective-permute-done | bytes 262176 | tf_op jit(solution)/shard_map/ppermute | solution.py:17
  68.3 5.3 collective-permute-start.8
  73.7 7.9 %collective-permute-done.1 = bf16[1024,128]{1,0:T(8,128)(2,1)S(1)} collective-permute-done((bf16[1024,128]{1,0:T(8,128)(2,1)S(1)}, bf16[1024,128]{1,0:T(8,128)(2,1)S(1)}, u32[]{:S(2)}, u32[]{:S(2)}) %collective-permute-start.1) | collective-permute-done | bytes 262176 | tf_op jit(solution)/shard_map/ppermute | solution.py:17
  81.6 5.3 collective-permute-start.9
  86.9 5.3 collective-permute-done.2
  92.2 4.3 collective-permute-done.9
  96.5 5.8 collective-permute-start.10
  102.3 7.1 collective-permute-done.3
  112.2 5.8 collective-permute-start.11
  118.0 4.4 collective-permute-done.4
  122.4 5.3 collective-permute-start.12
  127.8 5.2 collective-permute-done.5
  133.0 5.3 collective-permute-start.13
  138.3 4.4 collective-permute-done.6
  142.8 5.5 collective-permute-start.14
  148.4 4.4 collective-permute-done.7
  166.9 14.8 %reshape.171 = bf16[16,1024,1,2,64]{4,3,1,0,2:T(2,128)(2,1)} reshape(bf16[16384,128]{1,0:T(8,128)(2,1)} %constant_dynamic-slice_fusion) | data formatting | bytes 8388608 | tf_op jit(solution)/shard_map/reshape | solution.py:59
  181.6 20.1 %copy.39 = bf16[16,1024,1,2,64]{1,4,3,2,0:T(8,128)(2,1)} copy(bf16[16,1024,1,2,64]{4,3,1,0,2:T(2,128)(2,1)} %reshape.171) | data formatting | bytes 8388608
  201.7 14.8 %reshape.172 = bf16[16,1024,1,2,64]{4,3,1,0,2:T(2,128)(2,1)} reshape(bf16[16384,128]{1,0:T(8,128)(2,1)} %all-gather.5.cloned.1.call-done) | data formatting | bytes 8388608 | tf_op jit(solution)/shard_map/reshape | solution.py:59
  216.5 20.2 %copy.38 = bf16[16,1024,1,2,64]{1,4,3,2,0:T(8,128)(2,1)} copy(bf16[16,1024,1,2,64]{4,3,1,0,2:T(2,128)(2,1)} %reshape.172) | data formatting | bytes 8388608
  236.7 4.4 fusion.63
  241.0 169.4 %while.28 = (s32[]{:T(128)}, f32[1,2,512]{2,1,0:T(2,128)S(1)}, f32[1,2,512]{2,1,0:T(2,128)S(1)}, f32[512,1,2,64]{0,3,2,1:T(8,128)S(1)}, bf16[16,1024,1,2,64]{1,4...) while((s32[]{:T(128)}, f32[1,2,512]{2,1,0:T(2,128)S(1)}, ...), condition=%wide.region_5.6_spmd.clone, body=%wide.region_2.5_spmd.clone.sunk | while | flops 277026816 | bytes 14090341 | solution.py:111
  263.2 3.6 bitcast_reduce_fusion.2
  273.8 3.6 bitcast_reduce_fusion.2
  284.4 3.6 bitcast_reduce_fusion.2
  295.0 3.6 bitcast_reduce_fusion.2
  305.6 3.6 bitcast_reduce_fusion.2
  316.2 3.6 bitcast_reduce_fusion.2
  326.8 3.6 bitcast_reduce_fusion.2
  337.3 3.6 bitcast_reduce_fusion.2
  347.9 3.6 bitcast_reduce_fusion.2
  358.5 3.6 bitcast_reduce_fusion.2
  369.1 3.6 bitcast_reduce_fusion.2
  379.7 3.6 bitcast_reduce_fusion.2
  390.3 3.6 bitcast_reduce_fusion.2
  410.5 3.8 fusion.60
  414.3 3.9 convolution_convert_fusion.1
  421.3 227.2 %while.29 = (s32[]{:T(128)}, f32[512,1,2,64]{0,3,2,1:T(8,128)}, bf16[16384,128]{1,0:T(8,128)(2,1)}, bf16[16,1024,1,2,64]{1,4,3,2,0:T(8,128)(2,1)}, bf16[512,1,2,...) while((s32[]{:T(128)}, f32[512,1,2,64]{0,3,2,1:T(8,128)}, ...), condition=%wide.region_8.9_spmd.clone, body=%wide.region_7.8_spmd.clone.sunk | while | flops 679739392 | bytes 22687952 | solution.py:146
  655.7 67.9 %reduce-scatter.5.cloned.1.call-done = bf16[1024,128]{1,0:T(8,128)(2,1)} async-done(((bf16[16384,128]{1,0:T(8,128)(2,1)}), bf16[1024,128]{1,0:T(8,128)(2,1)}) %reduce-scatter.5.cloned.1.call-update) | async-done | bytes 262160 | tf_op jit(solution)/shard_map/reduce_scatter | solution.py:148
  723.6 4.3 all-to-all-start.1
  727.9 35.1 %reduce-scatter.3.cloned.1.call-done = bf16[64,4096]{1,0:T(8,128)(2,1)} async-done(((bf16[512,4096]{1,0:T(8,128)(2,1)}), bf16[64,4096]{1,0:T(8,128)(2,1)}) %reduce-scatter.3.cloned.1.call-update) | async-done | bytes 524304 | tf_op jit(solution)/shard_map/reduce_scatter | solution.py:160
  766.9 4.9 fusion.56
  (383 shorter events, 374.9 us)
Async XLA Ops:
  7.2 229.5 %copy-start = (bf16[4096,128]{1,0:T(8,128)(2,1)S(1)}, bf16[4096,128]{1,0:T(8,128)(2,1)}, u32[]{:S(2)}) copy-start(bf16[4096,128]{1,0:T(8,128)(2,1)} %param.17) | copy-start | bytes 3145732
  7.2 194.6 %all-gather.5.cloned.1.call-start = ((), (), s32[]{:S(2)}) async-start(), calls=%async_computation.5 | async-start | bytes 4456448 | tf_op jit(solution)/shard_map/all_gather | solution.py:92
  27.7 7.9 %copy-start.1 = (bf16[128,4096]{1,0:T(8,128)(2,1)S(1)}, bf16[128,4096]{1,0:T(8,128)(2,1)}, u32[]{:S(2)}) copy-start(bf16[128,4096]{1,0:T(8,128)(2,1)} %param.14) | copy-start | bytes 3145732
  27.7 8.2 %copy-start.15 = (f32[4096]{0:T(1024)S(1)}, f32[4096]{0:T(1024)}, u32[]{:S(2)}) copy-start(f32[4096]{0:T(1024)} %param.16) | copy-start | bytes 49156
  35.5 18.8 %copy-start.3 = (bf16[64,4096]{1,0:T(8,128)(2,1)S(1)}, bf16[64,4096]{1,0:T(8,128)(2,1)}, u32[]{:S(2)}) copy-start(bf16[64,4096]{1,0:T(8,128)(2,1)} %param.13) | copy-start | bytes 1572868
  35.5 19.0 %copy-start.13 = (f32[4096]{0:T(1024)S(1)}, f32[4096]{0:T(1024)}, u32[]{:S(2)}) copy-start(f32[4096]{0:T(1024)} %param.15) | copy-start | bytes 49156
  35.5 19.2 %copy-start.12 = (bf16[64,4096]{1,0:T(8,128)(2,1)S(1)}, bf16[64,4096]{1,0:T(8,128)(2,1)}, u32[]{:S(2)}) copy-start(bf16[64,4096]{1,0:T(8,128)(2,1)} %param.21) | copy-start | bytes 1572868
  54.2 103.6 %copy-start.5 = (bf16[128,8,128]{2,0,1:T(8,128)(2,1)S(1)}, bf16[128,8,128]{2,0,1:T(8,128)(2,1)}, u32[]{:S(2)}) copy-start(bf16[128,8,128]{2,0,1:T(8,128)(2,1)} %all_to_all.38) | copy-start | bytes 786436
  54.3 182.4 %all-gather.3.cloned.1.call-start = ((), (), s32[]{:S(2)}) async-start(), calls=%async_computation.4 | async-start | bytes 9437184 | tf_op jit(solution)/shard_map/all_gather | solution.py:26
  54.5 27.0 %copy-start.17 = (f32[64]{0:T(128)}, f32[64]{0:T(128)S(1)}, u32[]{:S(2)}) copy-start(f32[64]{0:T(128)S(1)} %add_rsqrt_fusion.1) | copy-start | bytes 772
  55.8 597.1 %all-reduce.2.cloned.1.call-start = ((), (), s32[]{:S(2)}) async-start(), calls=%async_computation.8 | async-start | bytes 2097152 | tf_op jit(solution)/shard_map/psum | solution.py:159
  55.9 12.4 %collective-permute-start = (bf16[1024,128]{1,0:T(8,128)(2,1)}, bf16[1024,128]{1,0:T(8,128)(2,1)S(1)}, u32[]{:S(2)}, u32[]{:S(2)}) collective-permute-start(bf16[1024,128]{1,0:T(8,128)(2,1)} %bitcast.254), channel_id=1, source_target_pairs={{0,8},{8,16},{16,24},{24,32},{32,40},{40,48},{48,56},{56,64},{64,7... | collective-permute-start | bytes 786440 | tf_op jit(solution)/shard_map/ppermute | solution.py:17
  68.3 13.2 %collective-permute-start.1 = (bf16[1024,128]{1,0:T(8,128)(2,1)S(1)}, bf16[1024,128]{1,0:T(8,128)(2,1)S(1)}, u32[]{:S(2)}, u32[]{:S(2)}) collective-permute-start(bf16[1024,128]{1,0:T(8,128)(2,1)S(1)} %collective-permute-done), channel_id=1, source_target_pairs={{0,8},{8,16},{16,24},{24,32},{32,40},{40,48},{48,56},{56,64},{64,7... | collective-permute-start | bytes 786440 | tf_op jit(solution)/shard_map/ppermute | solution.py:17
  68.3 13.2 %collective-permute-start.8 = (bf16[1024,128]{1,0:T(8,128)(2,1)}, bf16[1024,128]{1,0:T(8,128)(2,1)S(1)}, u32[]{:S(2)}, u32[]{:S(2)}) collective-permute-start(bf16[1024,128]{1,0:T(8,128)(2,1)} %bitcast.255), channel_id=1, source_target_pairs={{0,120},{8,0},{16,8},{24,16},{32,24},{40,32},{48,40},{56,48},{64,5... | collective-permute-start | bytes 786440 | tf_op jit(solution)/shard_map/ppermute | solution.py:19
  81.6 10.6 %collective-permute-start.2 = (bf16[1024,128]{1,0:T(8,128)(2,1)S(1)}, bf16[1024,128]{1,0:T(8,128)(2,1)S(1)}, u32[]{:S(2)}, u32[]{:S(2)}) collective-permute-start(bf16[1024,128]{1,0:T(8,128)(2,1)S(1)} %collective-permute-done.1), channel_id=1, source_target_pairs={{0,8},{8,16},{16,24},{24,32},{32,40},{40,48},{48,56},{56,64},{64,7... | collective-permute-start | bytes 786440 | tf_op jit(solution)/shard_map/ppermute | solution.py:17
  81.6 14.9 %collective-permute-start.9 = (bf16[1024,128]{1,0:T(8,128)(2,1)S(1)}, bf16[1024,128]{1,0:T(8,128)(2,1)S(1)}, u32[]{:S(2)}, u32[]{:S(2)}) collective-permute-start(bf16[1024,128]{1,0:T(8,128)(2,1)S(1)} %collective-permute-done.8), channel_id=1, source_target_pairs={{0,120},{8,0},{16,8},{24,16},{32,24},{40,32},{48,40},{56,48},{64,5... | collective-permute-start | bytes 786440 | tf_op jit(solution)/shard_map/ppermute | solution.py:19
  92.2 17.3 %collective-permute-start.3 = (bf16[1024,128]{1,0:T(8,128)(2,1)S(1)}, bf16[1024,128]{1,0:T(8,128)(2,1)S(1)}, u32[]{:S(2)}, u32[]{:S(2)}) collective-permute-start(bf16[1024,128]{1,0:T(8,128)(2,1)S(1)} %collective-permute-done.2), channel_id=1, source_target_pairs={{0,8},{8,16},{16,24},{24,32},{32,40},{40,48},{48,56},{56,64},{64,7... | collective-permute-start | bytes 786440 | tf_op jit(solution)/shard_map/ppermute | solution.py:17
  96.5 15.7 %collective-permute-start.10 = (bf16[1024,128]{1,0:T(8,128)(2,1)S(1)}, bf16[1024,128]{1,0:T(8,128)(2,1)S(1)}, u32[]{:S(2)}, u32[]{:S(2)}) collective-permute-start(bf16[1024,128]{1,0:T(8,128)(2,1)S(1)} %collective-permute-done.9), channel_id=1, source_target_pairs={{0,120},{8,0},{16,8},{24,16},{32,24},{40,32},{48,40},{56,48},{64,5... | collective-permute-start | bytes 786440 | tf_op jit(solution)/shard_map/ppermute | solution.py:19
  109.4 33.3 %copy-start.6 = (bf16[1024,128]{1,0:T(8,128)(2,1)}, bf16[1024,128]{1,0:T(8,128)(2,1)S(1)}, u32[]{:S(2)}) copy-start(bf16[1024,128]{1,0:T(8,128)(2,1)S(1)} %collective-permute-done.3) | copy-start | bytes 786436
  109.4 13.0 %collective-permute-start.4 = (bf16[1024,128]{1,0:T(8,128)(2,1)S(1)}, bf16[1024,128]{1,0:T(8,128)(2,1)S(1)}, u32[]{:S(2)}, u32[]{:S(2)}) collective-permute-start(bf16[1024,128]{1,0:T(8,128)(2,1)S(1)} %collective-permute-done.3), channel_id=1, source_target_pairs={{0,8},{8,16},{16,24},{24,32},{32,40},{40,48},{48,56},{56,64},{64,7... | collective-permute-start | bytes 786440 | tf_op jit(solution)/shard_map/ppermute | solution.py:17
  112.2 10.2 %collective-permute-start.11 = (bf16[1024,128]{1,0:T(8,128)(2,1)S(1)}, bf16[1024,128]{1,0:T(8,128)(2,1)S(1)}, u32[]{:S(2)}, u32[]{:S(2)}) collective-permute-start(bf16[1024,128]{1,0:T(8,128)(2,1)S(1)} %collective-permute-done.10), channel_id=1, source_target_pairs={{0,120},{8,0},{16,8},{24,16},{32,24},{40,32},{48,40},{56,48},{64,5... | collective-permute-start | bytes 786440 | tf_op jit(solution)/shard_map/ppermute | solution.py:19
  122.4 10.5 %copy-start.8 = (bf16[1024,128]{1,0:T(8,128)(2,1)}, bf16[1024,128]{1,0:T(8,128)(2,1)S(1)}, u32[]{:S(2)}) copy-start(bf16[1024,128]{1,0:T(8,128)(2,1)S(1)} %collective-permute-done.4) | copy-start | bytes 786436
  122.4 10.5 %collective-permute-start.5 = (bf16[1024,128]{1,0:T(8,128)(2,1)S(1)}, bf16[1024,128]{1,0:T(8,128)(2,1)S(1)}, u32[]{:S(2)}, u32[]{:S(2)}) collective-permute-start(bf16[1024,128]{1,0:T(8,128)(2,1)S(1)} %collective-permute-done.4), channel_id=1, source_target_pairs={{0,8},{8,16},{16,24},{24,32},{32,40},{40,48},{48,56},{56,64},{64,7... | collective-permute-start | bytes 786440 | tf_op jit(solution)/shard_map/ppermute | solution.py:17
  122.4 10.5 %collective-permute-start.12 = (bf16[1024,128]{1,0:T(8,128)(2,1)S(1)}, bf16[1024,128]{1,0:T(8,128)(2,1)}, u32[]{:S(2)}, u32[]{:S(2)}) collective-permute-start(bf16[1024,128]{1,0:T(8,128)(2,1)S(1)} %collective-permute-done.11), channel_id=1, source_target_pairs={{0,120},{8,0},{16,8},{24,16},{32,24},{40,32},{48,40},{56,48},{64,5... | collective-permute-start | bytes 786440 | tf_op jit(solution)/shard_map/ppermute | solution.py:19
  132.9 5.4 copy-start.10
  132.9 9.8 %collective-permute-start.6 = (bf16[1024,128]{1,0:T(8,128)(2,1)S(1)}, bf16[1024,128]{1,0:T(8,128)(2,1)}, u32[]{:S(2)}, u32[]{:S(2)}) collective-permute-start(bf16[1024,128]{1,0:T(8,128)(2,1)S(1)} %collective-permute-done.5), channel_id=1, source_target_pairs={{0,8},{8,16},{16,24},{24,32},{32,40},{40,48},{48,56},{56,64},{64,7... | collective-permute-start | bytes 786440 | tf_op jit(solution)/shard_map/ppermute | solution.py:17
  133.0 9.9 %collective-permute-start.13 = (bf16[1024,128]{1,0:T(8,128)(2,1)}, bf16[1024,128]{1,0:T(8,128)(2,1)}, u32[]{:S(2)}, u32[]{:S(2)}) collective-permute-start(bf16[1024,128]{1,0:T(8,128)(2,1)} %collective-permute-done.12), channel_id=1, source_target_pairs={{0,120},{8,0},{16,8},{24,16},{32,24},{40,32},{48,40},{56,48},{64,5... | collective-permute-start | bytes 786440 | tf_op jit(solution)/shard_map/ppermute | solution.py:19
  142.7 10.0 %collective-permute-start.7 = (bf16[1024,128]{1,0:T(8,128)(2,1)}, bf16[1024,128]{1,0:T(8,128)(2,1)}, u32[]{:S(2)}, u32[]{:S(2)}) collective-permute-start(bf16[1024,128]{1,0:T(8,128)(2,1)} %collective-permute-done.6), channel_id=1, source_target_pairs={{0,8},{8,16},{16,24},{24,32},{32,40},{40,48},{48,56},{56,64},{64,7... | collective-permute-start | bytes 786440 | tf_op jit(solution)/shard_map/ppermute | solution.py:17
  142.8 19.3 %copy-start.11 = (bf16[1024,128]{1,0:T(8,128)(2,1)S(1)}, bf16[1024,128]{1,0:T(8,128)(2,1)}, u32[]{:S(2)}) copy-start(bf16[1024,128]{1,0:T(8,128)(2,1)} %copy-done.10) | copy-start | bytes 786436
  142.8 19.4 %copy-start.9 = (bf16[1024,128]{1,0:T(8,128)(2,1)S(1)}, bf16[1024,128]{1,0:T(8,128)(2,1)}, u32[]{:S(2)}) copy-start(bf16[1024,128]{1,0:T(8,128)(2,1)} %copy-done.8) | copy-start | bytes 786436
  142.8 19.4 %copy-start.7 = (bf16[1024,128]{1,0:T(8,128)(2,1)S(1)}, bf16[1024,128]{1,0:T(8,128)(2,1)}, u32[]{:S(2)}) copy-start(bf16[1024,128]{1,0:T(8,128)(2,1)} %copy-done.6) | copy-start | bytes 786436
  142.8 17.3 %collective-permute-start.14 = (bf16[1024,128]{1,0:T(8,128)(2,1)}, bf16[1024,128]{1,0:T(8,128)(2,1)S(1)}, u32[]{:S(2)}, u32[]{:S(2)}) collective-permute-start(bf16[1024,128]{1,0:T(8,128)(2,1)} %collective-permute-done.13), channel_id=1, source_target_pairs={{0,120},{8,0},{16,8},{24,16},{32,24},{40,32},{48,40},{56,48},{64,5... | collective-permute-start | bytes 786440 | tf_op jit(solution)/shard_map/ppermute | solution.py:19
  241.0 169.4 %copy-start.19 = (bf16[128,4096]{1,0:T(8,128)(2,1)S(1)}, bf16[128,4096]{1,0:T(8,128)(2,1)}, u32[]{:S(2)}) copy-start(bf16[128,4096]{1,0:T(8,128)(2,1)} %param.20) | copy-start | bytes 3145732
  418.2 305.4 %reduce-scatter.5.cloned.1.call-start = ((), (), s32[]{:S(2)}) async-start(), calls=%async_computation.7 | async-start | bytes 4456448 | tf_op jit(solution)/shard_map/reduce_scatter | solution.py:148
  648.6 114.4 %copy-start.4 = (bf16[64,4096]{1,0:T(8,128)(2,1)S(1)}, bf16[64,4096]{1,0:T(8,128)(2,1)}, u32[]{:S(2)}) copy-start(bf16[64,4096]{1,0:T(8,128)(2,1)} %param.13) | copy-start | bytes 1572868
  648.6 114.4 %copy-start.14 = (f32[4096]{0:T(1024)S(1)}, f32[4096]{0:T(1024)}, u32[]{:S(2)}) copy-start(f32[4096]{0:T(1024)} %param.15) | copy-start | bytes 49156
  648.6 114.4 %reduce-scatter.3.cloned.1.call-start = ((), (), s32[]{:S(2)}) async-start(), calls=%async_computation.6 | async-start | bytes 4718592 | tf_op jit(solution)/shard_map/reduce_scatter | solution.py:160
  648.6 115.7 %copy-start.18 = (f32[64]{0:T(128)S(1)}, f32[64]{0:T(128)}, u32[]{:S(2)}) copy-start(f32[64]{0:T(128)} %copy-done.17) | copy-start | bytes 772
  649.7 117.2 %copy-start.2 = (bf16[128,4096]{1,0:T(8,128)(2,1)S(1)}, bf16[128,4096]{1,0:T(8,128)(2,1)}, u32[]{:S(2)}) copy-start(bf16[128,4096]{1,0:T(8,128)(2,1)} %param.14) | copy-start | bytes 3145732
  649.7 117.2 %copy-start.16 = (f32[4096]{0:T(1024)S(1)}, f32[4096]{0:T(1024)}, u32[]{:S(2)}) copy-start(f32[4096]{0:T(1024)} %param.16) | copy-start | bytes 49156
  723.6 43.1 %all-to-all-start.1 = ((bf16[8,128,128]{2,1,0:T(8,128)(2,1)}), bf16[8,128,128]{2,1,0:T(8,128)(2,1)S(1)}, u32[]{:S(2)}, u32[]{:S(2)}) async-start(bf16[8,128,128]{2,1,0:T(8,128)(2,1)} %bitcast.265), calls=%async_computation.3 | async-start | bytes 524288 | tf_op jit(solution)/shard_map/all_to_all | solution.py:152
Sparse Core Ops, SparseCore 0:
  54.4 65.9 all-gather.4
  122.7 48.8 all-gather.2
  418.3 83.8 all-reduce.1
  648.7 74.8 reduce-scatter.4
  725.9 37.0 reduce-scatter.2
